TPU v7x, 32 devices: a whole 2x2x4 slice. The times are simulated.
32 devices in a mesh: sp: 4 (over y, x), dp: 8 (over z, core).
Axes of the slice: x: 2, y: 2, z: 4, core: 2. Of those that a mesh axis runs over, the one named last changes fastest.
Arguments:
- tokens: bfloat16 [8, 1024, 2048], P('dp', 'sp'), may hold values from -200 to 200
- w_qdown: bfloat16 [2048, 512], P('dp'), may hold values from -0.125 to 0.125
- w_kvdown: bfloat16 [2048, 512], P('dp'), may hold values from -0.125 to 0.125
- w_rotary: bfloat16 [2048, 64], replicated, may hold values from -0.125 to 0.125
- q_gain: float32 [512], replicated, may hold values from 0.1 to 1.9
- kv_gain: float32 [512], replicated, may hold values from 0.1 to 1.9
- w_qup: bfloat16 [512, 3072], P('dp'), may hold values from -1 to 1
- w_kvup: bfloat16 [512, 4096], P('dp'), may hold values from -1 to 1
- w_out: bfloat16 [2048, 2048], P(None, 'dp'), may hold values from -0.125 to 0.125
- out_gain: float32 [2048], replicated, may hold values from 0.1 to 1.9
Outputs:
- mixed: bfloat16 [8, 1024, 2048], P('dp', 'sp')
All inputs are finite; a program needn't handle non-finite values.
Results may differ from a plain program's by a relative error of at most 0.01.
The roundings to bfloat16 on the way count: a program that leaves them out, or rounds other values in their place, can miss the bound.
Values may be sent and summed in bfloat16 or wider, within the bound.
A program may use at most 128 MiB of HBM per device.

v0:
```python
import math

import jax
import jax.numpy as jnp
from jax import lax
from jax.sharding import PartitionSpec as P

HEADS = 16
NOPE = 128
ROPE = 64
VDIM = 128


EPSILON = 1e-06
THETA = 10000.0


def norm_rows(values, gain):
    scale = lax.rsqrt(jnp.mean(values * values, axis=-1, keepdims=True) + EPSILON)
    return values * scale * gain


def rotate(values, cosine, sine):
    half = values.shape[-1] // 2
    first = values[..., :half]
    second = values[..., half:]
    return jnp.concatenate(
        [first * cosine - second * sine, second * cosine + first * sine], axis=-1
    )


def turn_tables(offset, count):
    positions = (offset + jnp.arange(count)).astype(jnp.float32)
    freqs = THETA ** (-jnp.arange(0, ROPE, 2).astype(jnp.float32) / ROPE)
    angles = positions[:, None] * freqs[None, :]
    return (jnp.cos(angles), jnp.sin(angles))


def make_queries(q_full, cosine, sine, heads_here):
    rows = q_full.shape[0]
    shaped = q_full.reshape(rows, heads_here, NOPE + ROPE)
    turned = rotate(shaped[..., NOPE:], cosine[:, None, :], sine[:, None, :])
    joined = jnp.concatenate([shaped[..., :NOPE], turned], axis=-1)
    return joined.reshape(rows, heads_here * (NOPE + ROPE)).astype(jnp.bfloat16)


def attend(query_heads, keyval_heads, key_rot, heads_here):
    length = query_heads.shape[0]
    block = math.gcd(length, 512)
    scaling = (NOPE + ROPE) ** (-0.5)
    queries = query_heads.reshape(length, heads_here, NOPE + ROPE)
    keyval = keyval_heads.reshape(length, heads_here, NOPE + VDIM)
    keys_all = keyval[..., :NOPE]
    values_all = keyval[..., NOPE:]
    outputs = []
    for begin in range(0, length, block):
        finish = begin + block
        query_block = queries[begin:finish]
        scores = jnp.einsum(
            "qhd,khd->hqk",
            query_block[..., :NOPE],
            keys_all[:finish],
            preferred_element_type=jnp.float32,
        )
        scores = scores + jnp.einsum(
            "qhd,kd->hqk",
            query_block[..., NOPE:],
            key_rot[:finish],
            preferred_element_type=jnp.float32,
        )
        scores = scores * scaling
        query_pos = begin + jnp.arange(block)
        key_pos = jnp.arange(finish)
        allowed = key_pos[None, :] <= query_pos[:, None]
        scores = jnp.where(allowed[None], scores, -jnp.inf)
        top = jnp.max(scores, axis=-1, keepdims=True)
        expo = jnp.exp(scores - top)
        weights = (expo / jnp.sum(expo, axis=-1, keepdims=True)).astype(jnp.bfloat16)
        attended = jnp.einsum(
            "hqk,khd->qhd", weights, values_all[:finish], preferred_element_type=jnp.float32
        )
        outputs.append(attended.astype(jnp.bfloat16))
    return jnp.concatenate(outputs, axis=0).reshape(length, heads_here * VDIM)


def body(tokens, w_qdown, w_kvdown, w_rotary, q_gain, kv_gain, w_qup, w_kvup, w_out, out_gain):
    own_rows = tokens[0]
    tok_count = own_rows.shape[0]
    sp_count = lax.axis_size("sp")
    sp_place = lax.axis_index("sp")
    length = tok_count * sp_count
    heads_here = HEADS // sp_count
    pieces = (
        lax.all_gather(w_qdown, "dp", axis=0, tiled=True),
        lax.all_gather(w_kvdown, "dp", axis=0, tiled=True),
    )
    q_lat = jnp.dot(own_rows, pieces[0], preferred_element_type=jnp.float32)
    kv_lat = jnp.dot(own_rows, pieces[1], preferred_element_type=jnp.float32)
    q_norm = norm_rows(q_lat, q_gain).astype(jnp.bfloat16)
    kv_norm = norm_rows(kv_lat, kv_gain).astype(jnp.bfloat16)
    own_cos, own_sin = turn_tables(sp_place * tok_count, tok_count)
    key_rot = rotate(
        jnp.dot(own_rows, w_rotary, preferred_element_type=jnp.float32), own_cos, own_sin
    ).astype(jnp.bfloat16)
    q_all, kv_all, rot_all = (
        lax.all_gather(q_norm, "sp", axis=0, tiled=True),
        lax.all_gather(kv_norm, "sp", axis=0, tiled=True),
        lax.all_gather(key_rot, "sp", axis=0, tiled=True),
    )
    q_width = heads_here * (NOPE + ROPE)
    kv_width = heads_here * (NOPE + VDIM)
    q_columns = lax.dynamic_slice_in_dim(w_qup, sp_place * q_width, q_width, 1)
    kv_columns = lax.dynamic_slice_in_dim(w_kvup, sp_place * kv_width, kv_width, 1)
    pieces = (
        lax.all_gather(q_columns, "dp", axis=0, tiled=True),
        lax.all_gather(kv_columns, "dp", axis=0, tiled=True),
    )
    q_full = jnp.dot(q_all, pieces[0], preferred_element_type=jnp.float32)
    kv_full = jnp.dot(kv_all, pieces[1], preferred_element_type=jnp.float32)
    all_cos, all_sin = turn_tables(0, length)
    query_heads = make_queries(q_full, all_cos, all_sin, heads_here)
    keyval_heads = kv_full.astype(jnp.bfloat16)
    attended = attend(query_heads, keyval_heads, rot_all, heads_here)
    merged = lax.all_to_all(attended, "sp", split_axis=0, concat_axis=1, tiled=True)
    proj = jnp.dot(
        merged, lax.all_gather(w_out, "dp", axis=1, tiled=True), preferred_element_type=jnp.float32
    )
    mixed = norm_rows(proj, out_gain).astype(jnp.bfloat16)
    return mixed[None]


def solution(mesh):
    in_specs = (
        P("dp", "sp", None),
        P("dp", None),
        P("dp", None),
        P(),
        P(),
        P(),
        P("dp", None),
        P("dp", None),
        P(None, "dp"),
        P(),
    )
    out_specs = P("dp", "sp", None)
    return jax.shard_map(body, mesh=mesh, in_specs=in_specs, out_specs=out_specs, check_vma=False)
```

profile of v0, /device:TPU:0, one launch (start us, length us, event | category | flops | bytes accessed | tf_op | source)
XLA Modules:
  0.0 248.7 jit_solution(12525613199316772031)
XLA Ops:
  8.1 32.8 %all-gather.13.cloned.1.call-done = bf16[2048,512]{1,0:T(8,128)(2,1)} async-done(((bf16[256,512]{1,0:T(8,128)(2,1)}), bf16[2048,512]{1,0:T(8,128)(2,1)}) %all-gather.13.cloned.1.call-update) | async-done | bytes 2097168 | tf_op jit(solution)/shard_map/all_gather | solution.py:94
  40.8 2.4 multiply_reduce_fusion.1
  43.3 0.9 multiply_convert_fusion.1
  44.2 1.6 constant_dynamic-slice_fusion.1
  45.8 25.2 %all-gather.7.cloned.1.call-done = bf16[2048,512]{1,0:T(8,128)(2,1)} async-done(((bf16[256,512]{1,0:T(8,128)(2,1)}), bf16[2048,512]{1,0:T(8,128)(2,1)}) %all-gather.7.cloned.1.call-update) | async-done | bytes 2097168 | tf_op jit(solution)/shard_map/all_gather | solution.py:95
  71.0 2.4 multiply_reduce_fusion.2
  73.4 0.8 multiply_convert_fusion.2
  75.5 10.3 %all_gather.30 = bf16[1024,64]{0,1:T(8,128)(2,1)S(1)} all-gather(bf16[256,64]{0,1:T(8,128)(2,1)S(1)} %pad_maximum_fusion.3), channel_id=1, replica_groups=mesh['sp'=4,'dp'=8] {'sp'}, dimensions={0}, use_global_device_ids=true | all-gather | bytes 163840 | tf_op jit(solution)/shard_map/all_gather | solution.py:108
  85.9 0.9 constant_dynamic-slice_fusion
  87.6 1.3 multiply_cosine_fusion
  88.8 1.2 iota_compare_fusion
  90.0 15.7 %all_gather.29 = bf16[512,768]{1,0:T(8,128)(2,1)S(1)} all-gather(bf16[64,768]{1,0:T(8,128)(2,1)S(1)} %constant_dynamic-slice_fusion), channel_id=1, replica_groups=mesh['sp'=4,'dp'=8] {'dp'}, dimensions={0}, use_global_device_ids=true | all-gather | bytes 884736 | tf_op jit(solution)/shard_map/all_gather | solution.py:115
  105.7 4.0 %fusion.45 = f32[1024,768]{0,1:T(8,128)} fusion(bf16[1024,512]{1,0:T(8,128)(2,1)} %all-gather.15.cloned.1.call-done, bf16[512,768]{1,0:T(8,128)(2,1)S(1)} %all_gather.29), kind=kOutput, calls=%fused_computation.80 | convolution fusion | flops 805306368 | bytes 4980736 | tf_op jit(solution)/shard_map/dot_general | solution.py:118
  109.7 3.3 %copy.16 = bf16[1024,4,192]{2,0,1:T(8,128)(2,1)S(1)} copy(f32[1024,4,192]{0,2,1:T(8,128)} %bitcast.55) | data formatting | bytes 4718592 | tf_op jit(solution)/shard_map/reshape | solution.py:41
  112.9 2.1 subtract_convert_fusion
  115.1 7.9 %all-gather.11.cloned.1.call-done = bf16[512,1024]{1,0:T(8,128)(2,1)} async-done(((bf16[64,1024]{1,0:T(8,128)(2,1)}), bf16[512,1024]{1,0:T(8,128)(2,1)}) %all-gather.11.cloned.1.call-update) | async-done | bytes 1048592 | tf_op jit(solution)/shard_map/all_gather | solution.py:116
  123.0 27.8 %all-gather.9.cloned.1.call-done = bf16[1024,512]{1,0:T(8,128)(2,1)} async-done(((bf16[256,512]{1,0:T(8,128)(2,1)}), bf16[1024,512]{1,0:T(8,128)(2,1)}) %all-gather.9.cloned.1.call-update) | async-done | bytes 1048592 | tf_op jit(solution)/shard_map/all_gather | solution.py:107
  150.8 2.8 %convolution_convert_fusion = bf16[1024,1024]{0,1:T(8,128)(2,1)S(1)} fusion(bf16[1024,512]{1,0:T(8,128)(2,1)} %all-gather.9.cloned.1.call-done, bf16[512,1024]{1,0:T(8,128)(2,1)} %all-gather.11.cloned.1.call-done), kind=kOutput, calls=%fused_computation.17 | convolution fusion | flops 1074790400 | bytes 4194304 | tf_op jit(solution)/shard_map/dot_general | solution.py:119
  155.1 1.0 fusion.5
  156.1 2.0 copy-done.2
  158.0 0.8 fusion.44
  158.8 6.5 %fusion.11 = bf16[512,4,128]{0,2,1:T(8,128)(2,1)} fusion(f32[4,512]{1,0:T(4,128)S(1)} %fusion.44, bf16[1024,4,256]{0,2,1:T(8,128)(2,1)} %bitcast.59, f32[4,512,512]{1,2,0:T(8,128)} %copy-done.2), kind=kOutput, calls=%fused_computation.21 | convolution fusion | flops 271845888 | bytes 9445376 | tf_op jit(solution)/shard_map/hqk,khd->qhd/dot_general | solution.py:79
  165.4 2.4 fusion.28
  167.7 1.8 fusion.3
  169.6 3.2 %copy-done.1 = f32[4,512,1024]{2,1,0:T(8,128)} copy-done((f32[4,512,1024]{2,1,0:T(8,128)}, f32[4,512,1024]{2,1,0:T(8,128)S(1)}, u32[]{:S(2)}) %copy-start.1) | copy-done | bytes 8388632
  172.8 2.0 fusion.43
  174.9 11.1 %fusion.10 = bf16[512,4,128]{0,2,1:T(8,128)(2,1)} fusion(f32[4,512]{1,0:T(4,128)S(1)} %fusion.43, bf16[1024,4,256]{0,2,1:T(8,128)(2,1)S(1)} %bitcast.61, f32[4,512,1024]{2,1,0:T(8,128)} %copy-done.1), kind=kOutput, calls=%fused_computation.20 | convolution fusion | flops 543427584 | bytes 18358272 | tf_op jit(solution)/shard_map/hqk,khd->qhd/dot_general | solution.py:79
  186.0 1.3 pad_maximum_fusion
  188.3 16.8 %all_to_all.19 = bf16[4,256,512]{1,2,0:T(8,128)(2,1)S(1)} all-to-all(bf16[4,256,512]{1,2,0:T(8,128)(2,1)S(1)} %copy.21), channel_id=1, replica_groups=mesh['sp'=4,'dp'=8] {'sp'}, dimensions={0} | all-to-all | bytes 2097152 | tf_op jit(solution)/shard_map/all_to_all | solution.py:124
  205.1 29.7 %all-gather.17.cloned.1.call-done = bf16[2048,2048]{1,0:T(8,128)(2,1)} async-done(((bf16[2048,256]{1,0:T(8,128)(2,1)}), bf16[2048,2048]{1,0:T(8,128)(2,1)}) %all-gather.17.cloned.1.call-update) | async-done | bytes 8388624 | tf_op jit(solution)/shard_map/all_gather | solution.py:126
  234.8 5.8 %multiply_reduce_fusion = (f32[256]{0:T(256)S(1)}, f32[256,2048]{1,0:T(8,128)S(1)}) fusion(bf16[256,2048]{0,1:T(8,128)(2,1)S(1)} %bitcast.57, bf16[2048,2048]{1,0:T(8,128)(2,1)} %all-gather.17.cloned.1.call-done), kind=kOutput, calls=%fused_computation.14 | convolution fusion | flops 2148531968 | bytes 11535360 | tf_op jit(solution)/shard_map/dot_general | solution.py:125
  240.6 1.2 fusion.12
  (51 shorter events, 6.0 us)
Async XLA Ops:
  6.5 34.3 %copy-start = (bf16[1,256,2048]{2,1,0:T(8,128)(2,1)S(1)}, bf16[1,256,2048]{2,1,0:T(8,128)(2,1)}, u32[]{:S(2)}) copy-start(bf16[1,256,2048]{2,1,0:T(8,128)(2,1)} %param.10) | copy-start | bytes 3145732
  6.5 36.7 %copy-start.11 = (f32[512]{0:T(512)S(1)}, f32[512]{0:T(512)}, u32[]{:S(2)}) copy-start(f32[512]{0:T(512)} %param.14) | copy-start | bytes 6148
  6.5 34.3 %all-gather.13.cloned.1.call-start = ((), (), s32[]{:S(2)}) async-start(), calls=%async_computation.4 | async-start | bytes 2359296 | tf_op jit(solution)/shard_map/all_gather | solution.py:94
  7.3 63.8 %all-gather.7.cloned.1.call-start = ((), (), s32[]{:S(2)}) async-start(), calls=%async_computation.1 | async-start | bytes 2359296 | tf_op jit(solution)/shard_map/all_gather | solution.py:95
  8.0 65.4 %copy-start.12 = (f32[512]{0:T(512)S(1)}, f32[512]{0:T(512)}, u32[]{:S(2)}) copy-start(f32[512]{0:T(512)} %param.15) | copy-start | bytes 6148
  8.0 97.7 %all-gather.15.cloned.1.call-start = ((), (), s32[]{:S(2)}) async-start(), calls=%async_computation.5 | async-start | bytes 1310720 | tf_op jit(solution)/shard_map/all_gather | solution.py:106
  43.2 31.7 %copy-start.9 = (bf16[2048,64]{0,1:T(8,128)(2,1)S(1)}, bf16[2048,64]{0,1:T(8,128)(2,1)}, u32[]{:S(2)}) copy-start(bf16[2048,64]{0,1:T(8,128)(2,1)} %param.13) | copy-start | bytes 786436
  44.1 78.9 %all-gather.11.cloned.1.call-start = ((), (), s32[]{:S(2)}) async-start(), calls=%async_computation.3 | async-start | bytes 1179648 | tf_op jit(solution)/shard_map/all_gather | solution.py:116
  45.8 105.0 %all-gather.9.cloned.1.call-start = ((), (), s32[]{:S(2)}) async-start(), calls=%async_computation.2 | async-start | bytes 1310720 | tf_op jit(solution)/shard_map/all_gather | solution.py:107
  74.3 160.5 %all-gather.17.cloned.1.call-start = ((), (), s32[]{:S(2)}) async-start(), calls=%async_computation.6 | async-start | bytes 9437184 | tf_op jit(solution)/shard_map/all_gather | solution.py:126
  153.7 1.3 copy-start.5
  153.7 1.3 copy-start.3
  153.7 1.4 copy-start.8
  156.1 2.0 copy-start.2
  165.4 2.4 copy-start.4
  165.4 2.4 copy-start.6
  169.6 3.2 %copy-start.1 = (f32[4,512,1024]{2,1,0:T(8,128)}, f32[4,512,1024]{2,1,0:T(8,128)S(1)}, u32[]{:S(2)}) copy-start(f32[4,512,1024]{2,1,0:T(8,128)S(1)} %fusion.3) | copy-start | bytes 25165828
  172.8 2.0 copy-start.7
  234.8 5.8 %copy-start.10 = (f32[2048]{0:T(1024)S(1)}, f32[2048]{0:T(1024)}, u32[]{:S(2)}) copy-start(f32[2048]{0:T(1024)} %param.19) | copy-start | bytes 24580
Sparse Core Ops, SparseCore 0:
  8.9 31.8 all-gather.12
  42.4 28.5 all-gather.6
  72.9 26.3 all-gather.14
  100.8 22.2 all-gather.10
  124.7 26.0 all-gather.8
  152.3 82.4 all-gather.16
where the time goes:
time: 249 us
  waiting for transfers between devices  125 us (50%)
  blocking collectives  42.8 us (17%)
  matrix products  41.4 us (17%)
  between operations  13.7 us (6%)
  other arithmetic  12.7 us (5%)
  local copies, waits for them, and re-layouts  12.5 us (5%)
    all_gather x1, waiting for transfers between devices, body(): lax.all_gather(w_qdown, 'dp', axis=0, tiled=True)  32.8 us
    all_gather x1, waiting for transfers between devices, body(): lax.all_gather(w_out, 'dp', axis=1, tiled=True)  29.7 us
    all_gather x1, waiting for transfers between devices, body(): lax.all_gather(kv_norm, 'sp', axis=0, tiled=True)  27.8 us
    all_gather x1, waiting for transfers between devices, body(): lax.all_gather(w_kvdown, 'dp', axis=0, tiled=True)  25.2 us
    dot_general x2, matrix products, attend(): jnp.einsum('hqk,khd->qhd', weights, values_all[:finish], preferred_elemen...  17.6 us
    all_to_all x1, blocking collectives, body(): lax.all_to_all(attended, 'sp', split_axis=0, concat_axis=1, tiled=True)  16.8 us
    all_gather x1, blocking collectives, body(): lax.all_gather(q_columns, 'dp', axis=0, tiled=True)  15.7 us
    all_gather x1, blocking collectives, body(): lax.all_gather(key_rot, 'sp', axis=0, tiled=True)  10.3 us
  transfers between devices with their start and end apart: 6, of which 5 were waited for; matrix products, arithmetic and copies ran while one was open for 21% of the time, Pallas kernels for 0%

commit v1 on v0

--- a/solution.py
+++ b/solution.py
@@ -1,8 +1,12 @@
+import functools
 import math
 
 import jax
 import jax.numpy as jnp
+import numpy as np
 from jax import lax
+from jax.experimental import pallas as pl
+from jax.experimental.pallas import tpu as pltpu
 from jax.sharding import PartitionSpec as P
 
 HEADS = 16
@@ -13,6 +17,9 @@
 
 EPSILON = 1e-06
 THETA = 10000.0
+LANES = 128
+SUBLANES = 16
+MESH = pl.DeviceIdType.MESH
 
 
 def norm_rows(values, gain):
@@ -83,7 +90,7 @@
     return jnp.concatenate(outputs, axis=0).reshape(length, heads_here * VDIM)
 
 
-def body(tokens, w_qdown, w_kvdown, w_rotary, q_gain, kv_gain, w_qup, w_kvup, w_out, out_gain):
+def plain_body(tokens, w_qdown, w_kvdown, w_rotary, q_gain, kv_gain, w_qup, w_kvup, w_out, out_gain):
     own_rows = tokens[0]
     tok_count = own_rows.shape[0]
     sp_count = lax.axis_size("sp")
@@ -129,6 +136,420 @@
     return mixed[None]
 
 
+def turn_table(length):
+    positions = np.arange(length, dtype=np.float32)
+    freqs = np.float32(THETA) ** (-np.arange(0, ROPE, 2).astype(np.float32) / np.float32(ROPE))
+    angles = positions[:, None] * freqs[None, :].astype(np.float32)
+    cosine, sine = np.cos(angles), np.sin(angles)
+    return np.concatenate([cosine, cosine, sine, sine], axis=1).astype(np.float32)
+
+
+class Copies:
+    def __init__(self, send_sems, recv_sems):
+        self.send_sems, self.recv_sems = send_sems, recv_sems
+        self.used = 0
+        self.sent = []
+
+    def start(self, source, target, device):
+        at = self.used
+        self.used += 1
+        copy = pltpu.make_async_remote_copy(
+            src_ref=source,
+            dst_ref=target,
+            send_sem=self.send_sems.at[at],
+            recv_sem=self.recv_sems.at[at],
+            device_id=device,
+            device_id_type=MESH,
+        )
+        copy.start()
+        self.sent.append(copy)
+        return copy
+
+
+class PlaneSpread:
+    def __init__(self, copies, place, view, rows):
+        self.copies, self.place, self.view, self.rows = copies, place, view, rows
+
+    def send(self):
+        me, rows = self.place["me"], self.rows
+        block = self.view(me, 0, rows)
+        self.along_x = self.copies.start(block, block, {"sp": self.place["x"]})
+        self.along_y = self.copies.start(block, block, {"sp": self.place["y"]})
+
+    def relay(self):
+        half = self.rows // 2
+        self.along_x.wait_recv()
+        block = self.view(self.place["x"], 0, half)
+        self.first = self.copies.start(block, block, {"sp": self.place["y"]})
+        self.along_y.wait_recv()
+        block = self.view(self.place["y"], half, half)
+        self.second = self.copies.start(block, block, {"sp": self.place["x"]})
+
+    def finish(self):
+        self.first.wait_recv()
+        self.second.wait_recv()
+
+
+class WeightGather:
+    def __init__(self, copies, place, source, buffer):
+        self.copies, self.place, self.source, self.buffer = copies, place, source, buffer
+        self.rows = source.shape[0] // place["sp_count"]
+
+    def piece(self, slot, owner, begin, count):
+        start = pl.multiple_of(owner * self.rows + begin, SUBLANES)
+        return self.buffer.at[slot, pl.ds(start, count), :]
+
+    def start(self):
+        place, rows = self.place, self.rows
+        own = self.source.at[pl.ds(pl.multiple_of(place["me"] * rows, SUBLANES), rows), :]
+        self.arrivals = []
+        for step in range(1, place["z_count"]):
+            target = self.piece(place["dp"], place["me"], 0, rows)
+            device = {"dp": lax.rem(place["dp"] + 2 * step, place["dp_count"])}
+            self.arrivals.append(self.copies.start(own, target, device))
+
+    def keep(self):
+        place = self.place
+        self.crossed = [
+            self.copies.start(self.source, self.buffer.at[place["dp"]], {"dp": place["core"]})
+        ]
+        self.buffer[place["dp"]] = self.source[...]
+
+    def slot(self, step):
+        place = self.place
+        return lax.rem(place["dp"] + place["dp_count"] - 2 * step, place["dp_count"])
+
+    def spread(self):
+        self.planes = []
+        for step in range(1, self.place["z_count"]):
+            self.arrivals[step - 1].wait_recv()
+            view = functools.partial(self.piece, self.slot(step))
+            plane = PlaneSpread(self.copies, self.place, view, self.rows)
+            plane.send()
+            self.planes.append(plane)
+
+    def relay(self):
+        for plane in self.planes:
+            plane.relay()
+
+    def cross(self):
+        for step in range(1, self.place["z_count"]):
+            self.planes[step - 1].finish()
+            block = self.buffer.at[self.slot(step)]
+            self.crossed.append(self.copies.start(block, block, {"dp": self.place["core"]}))
+
+    def finish(self):
+        for copy in self.crossed:
+            copy.wait_recv()
+
+
+class ColumnGather:
+    def __init__(self, copies, place, source, buffer):
+        self.copies, self.place, self.source, self.buffer = copies, place, source, buffer
+        width = buffer.shape[2]
+        self.columns = pl.ds(pl.multiple_of(place["me"] * width, LANES), width)
+
+    def start(self):
+        place = self.place
+        own = self.source.at[:, self.columns]
+        target = self.buffer.at[place["dp"]]
+        self.arrivals = []
+        for step in range(1, place["z_count"]):
+            device = {"dp": lax.rem(place["dp"] + 2 * step, place["dp_count"])}
+            self.arrivals.append(self.copies.start(own, target, device))
+
+    def keep(self):
+        place = self.place
+        own = self.source.at[:, self.columns]
+        target = self.buffer.at[place["dp"]]
+        self.crossed = [self.copies.start(own, target, {"dp": place["core"]})]
+        self.buffer[place["dp"]] = self.source[:, self.columns]
+
+    def cross(self):
+        place = self.place
+        for step in range(1, place["z_count"]):
+            self.arrivals[step - 1].wait_recv()
+            slot = lax.rem(place["dp"] + place["dp_count"] - 2 * step, place["dp_count"])
+            block = self.buffer.at[slot]
+            self.crossed.append(self.copies.start(block, block, {"dp": place["core"]}))
+
+    def finish(self):
+        for copy in self.crossed:
+            copy.wait_recv()
+
+
+def rotary_picks(rows, offset, skip):
+    width = skip + 2 * ROPE
+    row = lax.broadcasted_iota(jnp.int32, (rows, width), 0)
+    col = lax.broadcasted_iota(jnp.int32, (rows, width), 1)
+    half = ROPE // 2
+    minus = (col >= skip + ROPE) & (col < skip + ROPE + half)
+    origin = jnp.where(
+        col < skip + ROPE, col, jnp.where(minus, col - half, col - ROPE - half)
+    )
+    sign = jnp.where(minus, -1.0, 1.0)
+    return jnp.where(row == origin + offset, sign, 0.0).astype(jnp.bfloat16)
+
+
+def turned(values, table):
+    product = values * table
+    return product + pltpu.roll(product, ROPE, axis=1)
+
+
+def dot(left, right):
+    return jnp.dot(left, right, preferred_element_type=jnp.float32)
+
+
+def kernel(
+    sp_count, dp_count,
+    tokens, w_qdown, w_kvdown, w_rotary, q_gain, kv_gain, w_qup, w_kvup, w_out, out_gain, table,
+    out,
+    qd_all, kvd_all, qu_all, kvu_all, wo_all, q_lat, kv_lat,
+    q_heads, k_heads, v_heads, qu_laid, attended, merged, proj,
+    send_sems, recv_sems, back_send, back_recv,
+):
+    me = lax.axis_index("sp")
+    dp = lax.axis_index("dp")
+    place = {
+        "me": me,
+        "dp": dp,
+        "sp_count": sp_count,
+        "dp_count": dp_count,
+        "z_count": dp_count // 2,
+        "x": me + 1 - 2 * lax.rem(me, 2),
+        "y": lax.rem(me + 2, sp_count),
+        "core": dp + 1 - 2 * lax.rem(dp, 2),
+    }
+    count = tokens.shape[0]
+    heads = q_heads.shape[0]
+    rank = kvd_all.shape[2]
+
+    barrier = pltpu.get_barrier_semaphore()
+    peers = [{"sp": lax.rem(me + step, sp_count)} for step in range(1, sp_count)]
+    peers += [{"dp": lax.rem(dp + 2 * step, dp_count)} for step in range(1, dp_count // 2)]
+    peers += [{"dp": place["core"]}]
+    for peer in peers:
+        pl.semaphore_signal(barrier, inc=1, device_id=peer, device_id_type=MESH)
+    pl.semaphore_wait(barrier, len(peers))
+
+    copies = Copies(send_sems, recv_sems)
+    kvd = WeightGather(copies, place, w_kvdown, kvd_all)
+    qd = WeightGather(copies, place, w_qdown, qd_all)
+    kvu = ColumnGather(copies, place, w_kvup, kvu_all)
+    qu = ColumnGather(copies, place, w_qup, qu_all)
+    wo = WeightGather(copies, place, w_out, wo_all)
+    gathers = (kvd, qd, kvu, qu, wo)
+    for gather in gathers:
+        gather.start()
+    for gather in gathers:
+        gather.keep()
+
+    own_table = table[pl.ds(pl.multiple_of(me * count, SUBLANES), count), :]
+    rotary = dot(w_rotary[...], rotary_picks(ROPE, 0, 0)).astype(jnp.bfloat16)
+    key_rot = turned(dot(tokens[...], rotary), own_table)
+    lane = lax.broadcasted_iota(jnp.int32, key_rot.shape, 1)
+    key_rot = jnp.where(lane < ROPE, key_rot, 0.0).astype(jnp.bfloat16)
+    kv_lat[me, :, rank:] = key_rot
+
+    kvd.spread()
+    kvd.relay()
+    qd.spread()
+    kvd.cross()
+    qd.relay()
+    kvd.finish()
+    down = kvd_all[...].reshape(-1, rank)
+    kv_lat[me, :, :rank] = norm_rows(dot(tokens[...], down), kv_gain[...]).astype(jnp.bfloat16)
+
+    def block_view(buffer, owner, begin, rows):
+        return buffer.at[owner, pl.ds(begin, rows), :]
+
+    kv_plane = PlaneSpread(copies, place, functools.partial(block_view, kv_lat), count)
+    q_plane = PlaneSpread(copies, place, functools.partial(block_view, q_lat), count)
+    kv_plane.send()
+    qd.cross()
+    qd.finish()
+    down = qd_all[...].reshape(-1, qd_all.shape[2])
+    q_lat[me] = norm_rows(dot(tokens[...], down), q_gain[...]).astype(jnp.bfloat16)
+    q_plane.send()
+    kv_plane.relay()
+
+    qu.cross()
+    kvu.cross()
+    qu.finish()
+    laid = qu_all[...].reshape(-1, qu_all.shape[2])
+    head_width = NOPE + 2 * ROPE
+    for head in range(heads):
+        picks = rotary_picks(laid.shape[1], head * (NOPE + ROPE), NOPE)
+        qu_laid[:, head * head_width : (head + 1) * head_width] = dot(laid, picks).astype(
+            jnp.bfloat16
+        )
+    q_plane.relay()
+    wo.spread()
+    kvu.finish()
+    kv_plane.finish()
+
+    def make_keys(block, _):
+        rows = pl.ds(pl.multiple_of(block * count, SUBLANES), count)
+        latent = kv_lat[block]
+        full = dot(latent[:, :rank], kvu_all[...].reshape(rank, -1)).astype(jnp.bfloat16)
+        for head in range(heads):
+            at = head * (NOPE + VDIM)
+            k_heads[head, rows, :NOPE] = full[:, at : at + NOPE]
+            k_heads[head, rows, NOPE:] = latent[:, rank:]
+            v_heads[head, rows, :] = full[:, at + NOPE : at + NOPE + VDIM]
+        return 0
+
+    lax.fori_loop(0, sp_count, make_keys, 0)
+    q_plane.finish()
+
+    def make_block(block, _):
+        rows = pl.ds(pl.multiple_of(block * count, SUBLANES), count)
+        full = dot(q_lat[block], qu_laid[...])
+        turns = table[rows, :]
+        for head in range(heads):
+            at = head * head_width
+            q_heads[head, rows, :NOPE] = full[:, at : at + NOPE].astype(jnp.bfloat16)
+            part = full[:, at + NOPE : at + head_width]
+            q_heads[head, rows, NOPE:] = turned(part, turns).astype(jnp.bfloat16)
+        return 0
+
+    lax.fori_loop(0, sp_count, make_block, 0)
+    wo.relay()
+
+    factor = (NOPE + ROPE) ** (-0.5) * math.log2(math.e)
+    contract = (((1,), (1,)), ((), ()))
+    width = heads * VDIM
+
+    def back(block):
+        return pltpu.make_async_remote_copy(
+            src_ref=attended.at[block],
+            dst_ref=merged.at[:, pl.ds(pl.multiple_of(me * width, LANES), width)],
+            send_sem=back_send.at[block],
+            recv_sem=back_recv.at[me],
+            device_id={"sp": block},
+            device_id_type=MESH,
+        )
+
+    for block in reversed(range(sp_count)):
+        begin = block * count
+
+        def one_head(head, _):
+            query = q_heads[head, begin : begin + count, :]
+            near = lax.dot_general(
+                query, k_heads[head, begin : begin + count, :], contract,
+                preferred_element_type=jnp.float32,
+            )
+            row = lax.broadcasted_iota(jnp.int32, near.shape, 0)
+            col = lax.broadcasted_iota(jnp.int32, near.shape, 1)
+            near = jnp.where(col <= row, near, -jnp.inf)
+            top = jnp.max(near, axis=-1, keepdims=True)
+            if block:
+                far = lax.dot_general(
+                    query, k_heads[head, :begin, :], contract, preferred_element_type=jnp.float32
+                )
+                top = jnp.maximum(top, jnp.max(far, axis=-1, keepdims=True))
+            near = jnp.exp2((near - top) * factor)
+            total = jnp.sum(near, axis=-1, keepdims=True)
+            if block:
+                far = jnp.exp2((far - top) * factor)
+                total = total + jnp.sum(far, axis=-1, keepdims=True)
+            share = 1.0 / total
+            result = dot((near * share).astype(jnp.bfloat16), v_heads[head, begin : begin + count, :])
+            if block:
+                result = result + dot((far * share).astype(jnp.bfloat16), v_heads[head, :begin, :])
+            lanes = pl.ds(pl.multiple_of(head * VDIM, LANES), VDIM)
+            attended[block, :, lanes] = result.astype(jnp.bfloat16)
+            return 0
+
+        lax.fori_loop(0, heads, one_head, 0)
+
+        @pl.when(me != block)
+        def _():
+            back(block).start()
+
+        @pl.when(me == block)
+        def _():
+            merged[:, pl.ds(pl.multiple_of(me * width, LANES), width)] = attended[block]
+
+    wo.cross()
+    wo.finish()
+    for source in range(sp_count):
+
+        @pl.when(me != source)
+        def _():
+            pltpu.make_async_remote_copy(
+                src_ref=attended.at[source],
+                dst_ref=merged.at[:, source * width : (source + 1) * width],
+                send_sem=back_send.at[source],
+                recv_sem=back_recv.at[source],
+                device_id={"sp": source},
+                device_id_type=MESH,
+            ).wait()
+
+    out_width = wo_all.shape[2]
+
+    def project(piece, squares):
+        value = dot(merged[...], wo_all[piece])
+        proj[:, pl.ds(pl.multiple_of(piece * out_width, LANES), out_width)] = value
+        return squares + jnp.sum(value * value, axis=-1, keepdims=True)
+
+    squares = lax.fori_loop(0, dp_count, project, jnp.zeros((count, 1), jnp.float32))
+    scale = lax.rsqrt(squares * (1.0 / proj.shape[1]) + EPSILON)
+    out[...] = (proj[...] * scale * out_gain[...]).astype(jnp.bfloat16)
+    for copy in copies.sent:
+        copy.wait_send()
+
+
+def kernel_body(mesh, tokens, w_qdown, w_kvdown, w_rotary, q_gain, kv_gain, w_qup, w_kvup, w_out, out_gain):
+    sp_count, dp_count = mesh.shape["sp"], mesh.shape["dp"]
+    heads = HEADS // sp_count
+    count, depth = tokens.shape[1:]
+    length = count * sp_count
+    q_rank, kv_rank = w_qdown.shape[1], w_kvdown.shape[1]
+    bf16 = jnp.bfloat16
+    steps = dp_count // 2 - 1
+    sems = 3 * (6 * steps + 1) + 2 * (2 * steps + 1) + 2 * 4
+    sp_width = HEADS // sp_count
+    result = pl.pallas_call(
+        functools.partial(kernel, sp_count, dp_count),
+        out_shape=jax.ShapeDtypeStruct((count, w_out.shape[1] * dp_count), bf16),
+        in_specs=[pl.BlockSpec(memory_space=pltpu.VMEM)] * 11,
+        out_specs=pl.BlockSpec(memory_space=pltpu.VMEM),
+        scratch_shapes=[
+            pltpu.VMEM((dp_count,) + w_qdown.shape, bf16),
+            pltpu.VMEM((dp_count,) + w_kvdown.shape, bf16),
+            pltpu.VMEM((dp_count, w_qup.shape[0], sp_width * (NOPE + ROPE)), bf16),
+            pltpu.VMEM((dp_count, w_kvup.shape[0], sp_width * (NOPE + VDIM)), bf16),
+            pltpu.VMEM((dp_count,) + w_out.shape, bf16),
+            pltpu.VMEM((sp_count, count, q_rank), bf16),
+            pltpu.VMEM((sp_count, count, kv_rank + 2 * ROPE), bf16),
+            pltpu.VMEM((heads, length, NOPE + 2 * ROPE), bf16),
+            pltpu.VMEM((heads, length, NOPE + 2 * ROPE), bf16),
+            pltpu.VMEM((heads, length, VDIM), bf16),
+            pltpu.VMEM((q_rank, heads * (NOPE + 2 * ROPE)), bf16),
+            pltpu.VMEM((sp_count, count, heads * VDIM), bf16),
+            pltpu.VMEM((count, HEADS * VDIM), bf16),
+            pltpu.VMEM((count, w_out.shape[1] * dp_count), jnp.float32),
+            pltpu.SemaphoreType.DMA((sems,)),
+            pltpu.SemaphoreType.DMA((sems,)),
+            pltpu.SemaphoreType.DMA((sp_count,)),
+            pltpu.SemaphoreType.DMA((sp_count,)),
+        ],
+        compiler_params=pltpu.CompilerParams(
+            collective_id=0, has_side_effects=True, vmem_limit_bytes=60 * 1024 * 1024
+        ),
+        name="latent_attention",
+    )(
+        tokens[0], w_qdown, w_kvdown, w_rotary, q_gain[None], kv_gain[None], w_qup, w_kvup, w_out,
+        out_gain[None], jnp.asarray(turn_table(length)),
+    )
+    return result[None]
+
+
+def fits_kernel(mesh):
+    return mesh.shape["sp"] == 2 * 2 and mesh.shape["dp"] % 2 == 0
+
+
 def solution(mesh):
     in_specs = (
         P("dp", "sp", None),
@@ -143,4 +564,5 @@
         P(),
     )
     out_specs = P("dp", "sp", None)
+    body = functools.partial(kernel_body, mesh) if fits_kernel(mesh) else plain_body
     return jax.shard_map(body, mesh=mesh, in_specs=in_specs, out_specs=out_specs, check_vma=False)

time: 249 us -> 109 us (0.44)
  waiting for transfers between devices: 125 us -> 0 us
  Pallas kernels: 0 us -> 103 us
  blocking collectives: 42.8 us -> 0 us
  matrix products: 41.4 us -> 0 us
  between operations: 13.7 us -> 0.01 us
  other arithmetic: 12.7 us -> 0 us
  local copies, waits for them, and re-layouts: 12.5 us -> 4.26 us
    all_gather x6 -> x0, waiting for transfers between devices: 123 us -> none  [the longest x1 32.8 us: body(): lax.all_gather(w_qdown, 'dp', axis=0, tiled=True)]
    pallas_call x0 -> x1, Pallas kernels: none -> 103 us  [kernel_body(): pl.pallas_call(functools.partial(kernel, sp_count, dp_count), out_shape=j...]
    dot_general x12 -> x0, matrix products: 41.4 us -> none  [the longest x2 17.6 us: attend(): jnp.einsum('hqk,khd->qhd', weights, values_all[:finish], preferred_elemen...]
    all_gather x2 -> x0, blocking collectives: 26 us -> none  [the longest x1 15.7 us: body(): lax.all_gather(q_columns, 'dp', axis=0, tiled=True)]
    all_to_all x1 -> x0, blocking collectives: 16.8 us -> none  [body(): lax.all_to_all(attended, 'sp', split_axis=0, concat_axis=1, tiled=True)]
    reshape x1 -> x0, local copies, waits for them, and re-layouts: 3.26 us -> none  [make_queries(): shaped = q_full.reshape(rows, heads_here, NOPE + ROPE)]
    sub x2 -> x0, other arithmetic: 2.85 us -> none  [attend(): expo = jnp.exp(scores - top)]
    unnamed x26 -> x2, local copies, waits for them, and re-layouts: 5.87 us -> 4.26 us
  transfers between devices with their start and end apart: 6 -> 0, of which waited for: 5 -> 0; matrix products, arithmetic and copies ran while one was open for 21% -> 0% of each run, Pallas kernels for 0% -> 0%
where the time goes in v1:
time: 109 us; the launch traced here: 108 us
  Pallas kernels  103 us (94%)
  local copies, waits for them, and re-layouts  4.26 us (4%)
    pallas_call x1, Pallas kernels, kernel_body(): pl.pallas_call(functools.partial(kernel, sp_count, dp_count), out_shape=j...  103 us
    unnamed x2, local copies, waits for them, and re-layouts  4.26 us

profile of v1, /device:TPU:0, one launch (start us, length us, event | category | flops | bytes accessed | tf_op | source)
XLA Modules:
  0.0 107.7 jit_solution(5288519508916844868)
XLA Ops:
  0.0 2.0 %copy.12.w_rotary = bf16[2048,64]{1,0:T(8,128)(2,1)} copy(bf16[2048,64]{0,1:T(8,128)(2,1)} %param.14) | data formatting | bytes 524288 | tf_op args[3]
  2.0 103.4 %latent_attention.1 = bf16[256,2048]{1,0:T(8,128)(2,1)} custom-call(bf16[256,2048]{1,0:T(8,128)(2,1)} %bitcast.6, bf16[256,512]{1,0:T(8,128)(2,1)} %w_qdown.1, bf16[256,512]{1,0:T(8,128)(2,1)} %w_kvdown.1, bf16[2048,64]{1,0:T(8,128)(2,1)} %copy.12.w_rotary, f32[1,512]{1,0:T(1,128)} %bitcast.8, f32[1,512]{1,0:T(1,128)} %bitcast.9, bf16[64,3072]{1,0:T(8,128)(2,1)} %w_qup.1, ...), custom_call_target="tpu_custom_call" | custom-call | tf_op jit(solution)/shard_map/latent_attention/pallas_call | solution.py:513
  105.4 2.3 %copy.14 = bf16[1,256,2048]{2,1,0:T(8,128)(2,1)} copy(bf16[1,256,2048]{2,1,0:T(8,128)(2,1)} %bitcast.5) | data formatting | bytes 2097152

commit v2 on v1

--- a/solution.py
+++ b/solution.py
@@ -191,9 +191,12 @@
 
 
 class WeightGather:
-    def __init__(self, copies, place, source, buffer):
+    def __init__(self, copies, place, source, buffer, local_sem):
         self.copies, self.place, self.source, self.buffer = copies, place, source, buffer
         self.rows = source.shape[0] // place["sp_count"]
+        self.local_sem = local_sem
+        self.steps = range(1, place["z_count"])
+        self.planes = {}
 
     def piece(self, slot, owner, begin, count):
         start = pl.multiple_of(owner * self.rows + begin, SUBLANES)
@@ -202,50 +205,62 @@
     def start(self):
         place, rows = self.place, self.rows
         own = self.source.at[pl.ds(pl.multiple_of(place["me"] * rows, SUBLANES), rows), :]
-        self.arrivals = []
-        for step in range(1, place["z_count"]):
+        self.arrivals = {}
+        for step in self.steps:
             target = self.piece(place["dp"], place["me"], 0, rows)
             device = {"dp": lax.rem(place["dp"] + 2 * step, place["dp_count"])}
-            self.arrivals.append(self.copies.start(own, target, device))
+            self.arrivals[step] = self.copies.start(own, target, device)
 
     def keep(self):
         place = self.place
         self.crossed = [
             self.copies.start(self.source, self.buffer.at[place["dp"]], {"dp": place["core"]})
         ]
-        self.buffer[place["dp"]] = self.source[...]
+        self.local = None
+        if self.local_sem is None:
+            self.buffer[place["dp"]] = self.source[...]
+        else:
+            self.local = pltpu.make_async_copy(
+                self.source, self.buffer.at[place["dp"]], self.local_sem
+            )
+            self.local.start()
 
     def slot(self, step):
         place = self.place
         return lax.rem(place["dp"] + place["dp_count"] - 2 * step, place["dp_count"])
 
-    def spread(self):
-        self.planes = []
-        for step in range(1, self.place["z_count"]):
-            self.arrivals[step - 1].wait_recv()
-            view = functools.partial(self.piece, self.slot(step))
-            plane = PlaneSpread(self.copies, self.place, view, self.rows)
-            plane.send()
-            self.planes.append(plane)
-
-    def relay(self):
-        for plane in self.planes:
-            plane.relay()
-
-    def cross(self):
-        for step in range(1, self.place["z_count"]):
-            self.planes[step - 1].finish()
-            block = self.buffer.at[self.slot(step)]
-            self.crossed.append(self.copies.start(block, block, {"dp": self.place["core"]}))
+    def cross(self, step, owner):
+        block = self.piece(self.slot(step), owner, 0, self.rows)
+        self.crossed.append(self.copies.start(block, block, {"dp": self.place["core"]}))
+
+    def spread(self, step):
+        self.arrivals[step].wait_recv()
+        view = functools.partial(self.piece, self.slot(step))
+        plane = PlaneSpread(self.copies, self.place, view, self.rows)
+        plane.send()
+        self.planes[step] = plane
+        self.cross(step, self.place["me"])
+
+    def relay(self, step):
+        self.planes[step].relay()
+        self.cross(step, self.place["x"])
+        self.cross(step, self.place["y"])
+
+    def close(self, step):
+        self.planes[step].finish()
+        self.cross(step, self.place["far"])
 
     def finish(self):
+        if self.local is not None:
+            self.local.wait()
         for copy in self.crossed:
             copy.wait_recv()
 
 
 class ColumnGather:
-    def __init__(self, copies, place, source, buffer):
+    def __init__(self, copies, place, source, buffer, local_sem):
         self.copies, self.place, self.source, self.buffer = copies, place, source, buffer
+        self.local_sem = local_sem
         width = buffer.shape[2]
         self.columns = pl.ds(pl.multiple_of(place["me"] * width, LANES), width)
 
@@ -263,7 +278,8 @@
         own = self.source.at[:, self.columns]
         target = self.buffer.at[place["dp"]]
         self.crossed = [self.copies.start(own, target, {"dp": place["core"]})]
-        self.buffer[place["dp"]] = self.source[:, self.columns]
+        self.local = pltpu.make_async_copy(own, target, self.local_sem)
+        self.local.start()
 
     def cross(self):
         place = self.place
@@ -274,6 +290,7 @@
             self.crossed.append(self.copies.start(block, block, {"dp": place["core"]}))
 
     def finish(self):
+        self.local.wait()
         for copy in self.crossed:
             copy.wait_recv()
 
@@ -305,8 +322,8 @@
     tokens, w_qdown, w_kvdown, w_rotary, q_gain, kv_gain, w_qup, w_kvup, w_out, out_gain, table,
     out,
     qd_all, kvd_all, qu_all, kvu_all, wo_all, q_lat, kv_lat,
-    q_heads, k_heads, v_heads, qu_laid, attended, merged, proj,
-    send_sems, recv_sems, back_send, back_recv,
+    q_heads, k_heads, v_heads, qu_laid, attended, merged,
+    send_sems, recv_sems, back_send, back_recv, local_sems,
 ):
     me = lax.axis_index("sp")
     dp = lax.axis_index("dp")
@@ -318,6 +335,7 @@
         "z_count": dp_count // 2,
         "x": me + 1 - 2 * lax.rem(me, 2),
         "y": lax.rem(me + 2, sp_count),
+        "far": sp_count - 1 - me,
         "core": dp + 1 - 2 * lax.rem(dp, 2),
     }
     count = tokens.shape[0]
@@ -333,11 +351,11 @@
     pl.semaphore_wait(barrier, len(peers))
 
     copies = Copies(send_sems, recv_sems)
-    kvd = WeightGather(copies, place, w_kvdown, kvd_all)
-    qd = WeightGather(copies, place, w_qdown, qd_all)
-    kvu = ColumnGather(copies, place, w_kvup, kvu_all)
-    qu = ColumnGather(copies, place, w_qup, qu_all)
-    wo = WeightGather(copies, place, w_out, wo_all)
+    kvd = WeightGather(copies, place, w_kvdown, kvd_all, None)
+    qd = WeightGather(copies, place, w_qdown, qd_all, None)
+    kvu = ColumnGather(copies, place, w_kvup, kvu_all, local_sems.at[0])
+    qu = ColumnGather(copies, place, w_qup, qu_all, local_sems.at[1])
+    wo = WeightGather(copies, place, w_out, wo_all, local_sems.at[2])
     gathers = (kvd, qd, kvu, qu, wo)
     for gather in gathers:
         gather.start()
@@ -345,17 +363,27 @@
         gather.keep()
 
     own_table = table[pl.ds(pl.multiple_of(me * count, SUBLANES), count), :]
-    rotary = dot(w_rotary[...], rotary_picks(ROPE, 0, 0)).astype(jnp.bfloat16)
-    key_rot = turned(dot(tokens[...], rotary), own_table)
+    picks = rotary_picks(ROPE, 0, 0)
+    rotary = lax.dot_general(
+        picks, w_rotary[...], (((0,), (0,)), ((), ())), preferred_element_type=jnp.float32
+    ).astype(jnp.bfloat16)
+    key_rot = lax.dot_general(
+        tokens[...], rotary, (((1,), (1,)), ((), ())), preferred_element_type=jnp.float32
+    )
+    key_rot = turned(key_rot, own_table)
     lane = lax.broadcasted_iota(jnp.int32, key_rot.shape, 1)
     key_rot = jnp.where(lane < ROPE, key_rot, 0.0).astype(jnp.bfloat16)
     kv_lat[me, :, rank:] = key_rot
 
-    kvd.spread()
-    kvd.relay()
-    qd.spread()
-    kvd.cross()
-    qd.relay()
+    steps = kvd.steps
+    for step in steps:
+        kvd.spread(step)
+    for step in steps:
+        kvd.relay(step)
+        qd.spread(step)
+    for step in steps:
+        kvd.close(step)
+        qd.relay(step)
     kvd.finish()
     down = kvd_all[...].reshape(-1, rank)
     kv_lat[me, :, :rank] = norm_rows(dot(tokens[...], down), kv_gain[...]).astype(jnp.bfloat16)
@@ -366,7 +394,8 @@
     kv_plane = PlaneSpread(copies, place, functools.partial(block_view, kv_lat), count)
     q_plane = PlaneSpread(copies, place, functools.partial(block_view, q_lat), count)
     kv_plane.send()
-    qd.cross()
+    for step in steps:
+        qd.close(step)
     qd.finish()
     down = qd_all[...].reshape(-1, qd_all.shape[2])
     q_lat[me] = norm_rows(dot(tokens[...], down), q_gain[...]).astype(jnp.bfloat16)
@@ -384,7 +413,6 @@
             jnp.bfloat16
         )
     q_plane.relay()
-    wo.spread()
     kvu.finish()
     kv_plane.finish()
 
@@ -401,6 +429,7 @@
 
     lax.fori_loop(0, sp_count, make_keys, 0)
     q_plane.finish()
+    wo.spread(1)
 
     def make_block(block, _):
         rows = pl.ds(pl.multiple_of(block * count, SUBLANES), count)
@@ -414,7 +443,10 @@
         return 0
 
     lax.fori_loop(0, sp_count, make_block, 0)
-    wo.relay()
+
+    chores = [functools.partial(wo.spread, step) for step in steps if step > 1]
+    chores += [functools.partial(wo.relay, step) for step in steps]
+    chores_now = -(-len(chores) // sp_count)
 
     factor = (NOPE + ROPE) ** (-0.5) * math.log2(math.e)
     contract = (((1,), (1,)), ((), ()))
@@ -471,7 +503,12 @@
         def _():
             merged[:, pl.ds(pl.multiple_of(me * width, LANES), width)] = attended[block]
 
-    wo.cross()
+        for chore in chores[:chores_now]:
+            chore()
+        del chores[:chores_now]
+
+    for step in steps:
+        wo.close(step)
     wo.finish()
     for source in range(sp_count):
 
@@ -489,13 +526,14 @@
     out_width = wo_all.shape[2]
 
     def project(piece, squares):
+        lanes = pl.ds(pl.multiple_of(piece * out_width, LANES), out_width)
         value = dot(merged[...], wo_all[piece])
-        proj[:, pl.ds(pl.multiple_of(piece * out_width, LANES), out_width)] = value
+        out[:, lanes] = value
         return squares + jnp.sum(value * value, axis=-1, keepdims=True)
 
     squares = lax.fori_loop(0, dp_count, project, jnp.zeros((count, 1), jnp.float32))
-    scale = lax.rsqrt(squares * (1.0 / proj.shape[1]) + EPSILON)
-    out[...] = (proj[...] * scale * out_gain[...]).astype(jnp.bfloat16)
+    scale = lax.rsqrt(squares * (1.0 / out.shape[1]) + EPSILON)
+    out[...] = out[...] * scale * out_gain[...]
     for copy in copies.sent:
         copy.wait_send()
 
@@ -508,13 +546,14 @@
     q_rank, kv_rank = w_qdown.shape[1], w_kvdown.shape[1]
     bf16 = jnp.bfloat16
     steps = dp_count // 2 - 1
-    sems = 3 * (6 * steps + 1) + 2 * (2 * steps + 1) + 2 * 4
+    sems = 3 * (9 * steps + 1) + 2 * (2 * steps + 1) + 2 * 4
+    vmem, hbm = pl.BlockSpec(memory_space=pltpu.VMEM), pl.BlockSpec(memory_space=pl.ANY)
     sp_width = HEADS // sp_count
-    result = pl.pallas_call(
+    mixed = pl.pallas_call(
         functools.partial(kernel, sp_count, dp_count),
-        out_shape=jax.ShapeDtypeStruct((count, w_out.shape[1] * dp_count), bf16),
-        in_specs=[pl.BlockSpec(memory_space=pltpu.VMEM)] * 11,
-        out_specs=pl.BlockSpec(memory_space=pltpu.VMEM),
+        out_shape=jax.ShapeDtypeStruct((count, w_out.shape[1] * dp_count), jnp.float32),
+        in_specs=[vmem] * 6 + [hbm] * 3 + [vmem] * 2,
+        out_specs=vmem,
         scratch_shapes=[
             pltpu.VMEM((dp_count,) + w_qdown.shape, bf16),
             pltpu.VMEM((dp_count,) + w_kvdown.shape, bf16),
@@ -529,21 +568,21 @@
             pltpu.VMEM((q_rank, heads * (NOPE + 2 * ROPE)), bf16),
             pltpu.VMEM((sp_count, count, heads * VDIM), bf16),
             pltpu.VMEM((count, HEADS * VDIM), bf16),
-            pltpu.VMEM((count, w_out.shape[1] * dp_count), jnp.float32),
             pltpu.SemaphoreType.DMA((sems,)),
             pltpu.SemaphoreType.DMA((sems,)),
             pltpu.SemaphoreType.DMA((sp_count,)),
             pltpu.SemaphoreType.DMA((sp_count,)),
+            pltpu.SemaphoreType.DMA((3,)),
         ],
         compiler_params=pltpu.CompilerParams(
             collective_id=0, has_side_effects=True, vmem_limit_bytes=60 * 1024 * 1024
         ),
         name="latent_attention",
     )(
-        tokens[0], w_qdown, w_kvdown, w_rotary, q_gain[None], kv_gain[None], w_qup, w_kvup, w_out,
+        tokens[0], w_qdown, w_kvdown, w_rotary.T, q_gain[None], kv_gain[None], w_qup, w_kvup, w_out,
         out_gain[None], jnp.asarray(turn_table(length)),
     )
-    return result[None]
+    return mixed.astype(bf16)[None]
 
 
 def fits_kernel(mesh):

time: 109 us -> 111 us (1.018)
  the two profiles are of different devices: /device:TPU:0 before, /device:TPU:11 now
where the time goes in v2:
time: 111 us
  Pallas kernels  108 us (97%)
  other arithmetic  2.71 us (2%)
    pallas_call x1, Pallas kernels, kernel_body(): pl.pallas_call(functools.partial(kernel, sp_count, dp_count), out_shape=j...  108 us
    broadcast_in_dim x1, other arithmetic, kernel_body(): return mixed.astype(bf16)[None]  2.71 us

profile of v2, /device:TPU:11, one launch (start us, length us, event | category | flops | bytes accessed | tf_op | source)
XLA Modules:
  0.0 110.6 jit_solution(4075354662144787518)
XLA Ops:
  0.0 107.8 %latent_attention.1 = f32[256,2048]{1,0:T(8,128)} custom-call(bf16[256,2048]{1,0:T(8,128)(2,1)} %bitcast.7, bf16[256,512]{1,0:T(8,128)(2,1)} %w_qdown.1, bf16[256,512]{1,0:T(8,128)(2,1)} %w_kvdown.1, bf16[64,2048]{1,0:T(8,128)(2,1)} %bitcast.8, f32[1,512]{1,0:T(1,128)} %bitcast.10, f32[1,512]{1,0:T(1,128)} %bitcast.11, bf16[64,3072]{1,0:T(8,128)(2,1)} %w_qup.1, ...), custom_call_target="tpu_custom_call" | custom-call | tf_op jit(solution)/shard_map/latent_attention/pallas_call | solution.py:552
  107.8 2.7 %convert_bitcast_fusion = bf16[1,256,2048]{2,1,0:T(8,128)(2,1)} fusion(f32[256,2048]{1,0:T(8,128)} %latent_attention.1), kind=kLoop, calls=%fused_computation | loop fusion | flops 524288 | bytes 3145728 | tf_op jit(solution)/shard_map/broadcast_in_dim | solution.py:585
